TPU v7x, 32 devices: a whole 2x2x4 slice. The times are simulated.
32 devices in a mesh: grp: 2 (over y), ep: 8 (over z, core), tp: 2 (over x).
Axes of the slice: x: 2, y: 2, z: 4, core: 2. Of those that a mesh axis runs over, the one named last changes fastest.
Arguments:
- value_in: bfloat16 [8192, 1024], P(('grp', 'ep'), 'tp'), parts along dimension 0, may hold values from -6 to 6
- gate_in: bfloat16 [8192, 1024], P(('grp', 'ep'), 'tp'), parts along dimension 0, may hold values from -6 to 6
- conv_taps: float32 [31, 1024], P(None, 'tp'), may hold values from -12 to 12
- chan_gain: float32 [1024], replicated, may hold values from 0.1 to 1.9
- out_weight: bfloat16 [1024, 2048], P(None, 'tp'), may hold values from -0.1875 to 0.1875
- second_rows: bfloat16 [2048, 2048], P(('grp', 'ep')), parts along dimension 0, may hold values from -6 to 6
- expert_gain: float32 [2048], replicated, may hold values from 0.1 to 1.9
- routes: int32 [2048, 2], P(('grp', 'ep')), parts along dimension 0, may hold values from 0 to 3, all different within a row; in each aligned block of 128 rows (0 to 127, 128 to 255, ...) at most 96 rows name the same one
- route_weights: float32 [2048, 2], P(('grp', 'ep')), parts along dimension 0, may hold values from 0.1 to 0.9
- gate_w: bfloat16 [8, 2048, 2048], P('ep', None, 'tp'), may hold values from -0.125 to 0.125
- up_w: bfloat16 [8, 2048, 2048], P('ep', None, 'tp'), may hold values from -0.125 to 0.125
- down_w: bfloat16 [8, 2048, 2048], P('ep', 'tp'), may hold values from -0.125 to 0.125
Outputs:
- mixer_rows: bfloat16 [8192, 2048], P(('grp', 'ep'), 'tp'), parts along dimension 0
- routed_rows: bfloat16 [2048, 2048], P(('grp', 'ep'), 'tp'), parts along dimension 0
There are 2 independent parts, one for each index of `grp`. A program takes and returns all parts, laid end to end along the dimension named above; an argument that names none is the same for every part. Nothing has to cross between parts.
Inputs may be any that keep to these rules, and one draw needn't show every extreme that they name: `routes`: in each aligned block of 128 rows (the rows of one index of ep) no expert is named by more than 96 rows, a bound that some block reaches; each row names 2 different experts.
All inputs are finite; a program needn't handle non-finite values.
Results may differ from a plain program's by a relative error of at most 0.017.
Values may be sent and summed in bfloat16 or wider, within the bound.
A program may use at most 64 MiB of HBM per device.

v0:
```python
import jax
import jax.numpy as jnp
from jax import lax
from jax.sharding import PartitionSpec as P

eps = 1e-06


def partner_2(value, axis, bit):
    return lax.ppermute(value, axis, [(i, i ^ 1 << bit) for i in range(lax.axis_size(axis))])


def shifted(value, axis, by):
    devices = lax.axis_size(axis)
    pairs = [(i, i + by) for i in range(devices) if 0 <= i + by < devices]
    return lax.ppermute(value, axis, pairs)


def partner(block):
    return partner_2(block, "ep", 0)


def across(block):
    return lax.all_to_all(block, "ep", split_axis=0, concat_axis=0, tiled=True)


def on_device(
    value_in,
    gate_in,
    conv_taps,
    chan_gain,
    out_weight,
    second_rows,
    expert_gain,
    routes,
    route_weights,
    gate_w,
    up_w,
    down_w,
):
    taps = conv_taps.shape[0]
    glu = (value_in.astype(jnp.float32) * jax.nn.sigmoid(gate_in.astype(jnp.float32))).astype(
        jnp.bfloat16
    )
    length = glu.shape[0]
    before = shifted(glu[length - taps + 1 :], "ep", 1)
    padded = jnp.concatenate([before, glu], axis=0).astype(jnp.float32)
    total = jnp.zeros(glu.shape, jnp.float32)
    for offset in range(taps):
        total = total + conv_taps[offset][None, :] * padded[offset : offset + length]
    convolved = total.astype(jnp.bfloat16)
    channels = lax.all_gather(convolved, "tp", axis=1, tiled=True)
    values = channels.astype(jnp.float32)
    centered = values - jnp.mean(values, axis=-1, keepdims=True)
    scaled = (
        centered
        * lax.rsqrt(jnp.mean(centered * centered, axis=-1, keepdims=True) + eps)
        * chan_gain
    )
    activated = jax.nn.silu(scaled).astype(jnp.bfloat16)
    mixer_rows = jnp.dot(activated, out_weight, preferred_element_type=jnp.float32).astype(
        jnp.bfloat16
    )
    n_ep = lax.axis_size("ep")
    experts = n_ep // 2
    tokens = second_rows.shape[0]
    top = routes.shape[1]
    width = second_rows.shape[1]
    capacity = 2 * max(1, min(tokens // 2, 3 * tokens * top // (4 * experts)))
    half_slots = capacity // 2
    rows = second_rows.astype(jnp.float32)
    normed = (
        rows * lax.rsqrt(jnp.mean(rows * rows, axis=-1, keepdims=True) + eps) * expert_gain
    ).astype(jnp.bfloat16)
    chosen = routes.reshape(-1)
    hits = (chosen[:, None] == jnp.arange(experts, dtype=jnp.int32)[None, :]).astype(jnp.int32)
    place = jnp.sum((jnp.cumsum(hits, axis=0) - 1) * hits, axis=1)
    target = (chosen * capacity + place).reshape(tokens, top)
    slots = jnp.arange(experts * capacity, dtype=jnp.int32)
    matches = target[:, :, None] == slots[None, None, :]
    picker = jnp.any(matches, axis=1).astype(jnp.bfloat16)
    outgoing = jnp.dot(picker.T, normed, preferred_element_type=jnp.float32).astype(jnp.bfloat16)
    combiner = jnp.sum(jnp.where(matches, route_weights[:, :, None], 0.0), axis=1)
    upper = lax.axis_index("ep") % 2
    arrived = across(outgoing.reshape(n_ep, half_slots, width))
    other = partner(arrived)
    first = jnp.where(upper == 0, arrived, other)
    second = jnp.where(upper == 0, other, arrived)
    incoming = jnp.concatenate([first, second], axis=1)
    block_rows = incoming.reshape(n_ep * capacity, width)
    gate = jnp.dot(block_rows, gate_w[0], preferred_element_type=jnp.float32)
    lifted = jnp.dot(block_rows, up_w[0], preferred_element_type=jnp.float32)
    hidden = (jax.nn.silu(gate) * lifted).astype(jnp.bfloat16)
    partial_value = jnp.dot(hidden, down_w[0], preferred_element_type=jnp.float32)
    half_sums = lax.psum_scatter(
        partial_value.astype(jnp.bfloat16), "tp", scatter_dimension=1, tiled=True
    )
    columns = half_sums.shape[1]
    half_sums = half_sums.reshape(n_ep, capacity, columns)
    other_sums = partner(half_sums)
    joined = (half_sums.astype(jnp.float32) + other_sums.astype(jnp.float32)).astype(jnp.bfloat16)
    own = lax.dynamic_slice_in_dim(joined, upper * half_slots, half_slots, 1)
    results = across(own).reshape(experts * capacity, columns)
    routed_rows = jnp.dot(
        combiner,
        results.astype(jnp.float32),
        precision=lax.Precision.HIGHEST,
        preferred_element_type=jnp.float32,
    ).astype(jnp.bfloat16)
    return (mixer_rows, routed_rows)


def solution(mesh):
    placed = (
        P(("grp", "ep"), "tp"),
        P(("grp", "ep"), "tp"),
        P(None, "tp"),
        P(),
        P(None, "tp"),
        P(("grp", "ep"), None),
        P(),
        P(("grp", "ep"), None),
        P(("grp", "ep"), None),
        P("ep", None, "tp"),
        P("ep", None, "tp"),
        P("ep", "tp", None),
    )
    return jax.shard_map(
        on_device,
        mesh=mesh,
        in_specs=placed,
        out_specs=(P(("grp", "ep"), "tp"), P(("grp", "ep"), "tp")),
        check_vma=False,
    )
```

profile of v0, /device:TPU:0, one launch (start us, length us, event | category | flops | bytes accessed | tf_op | source)
XLA Modules:
  0.0 162.1 jit_solution(18409859760908548096)
XLA Ops:
  7.2 0.9 copy.32
  8.2 0.1 eq.48
  8.3 0.1 eq.44
  8.4 1.2 reduce-window.6
  10.1 0.1 reduce_sum.50
  10.3 0.7 multiply_add_fusion
  11.1 1.2 fusion.22
  12.4 1.7 %convolution_convert_fusion = bf16[384,2048]{1,0:T(8,128)(2,1)S(1)} fusion(pred[128,384]{1,0:T(8,128)(4,1)S(1)} %fusion.63, bf16[128,2048]{1,0:T(8,128)(2,1)} %param.17, f32[2048]{0:T(1024)} %param.18, f32[128]{0:T(128)S(1)} %add_rsqrt_fusion.1), kind=kOutput, calls=%fused_computation.9 | convolution fusion | flops 203161600 | bytes 2155008 | tf_op jit(solution)/shard_map/dot_general | solution.py:82
  14.1 44.1 %all_to_all.10 = bf16[8,48,2048]{2,1,0:T(8,128)(2,1)} all-to-all(bf16[8,48,2048]{2,1,0:T(8,128)(2,1)S(1)} %bitcast.70), channel_id=1, replica_groups=mesh['grp'=2,'ep'=8,'tp'=2] {'ep'}, dimensions={0} | all-to-all | bytes 3145728 | tf_op jit(solution)/shard_map/all_to_all | solution.py:24
  58.1 3.7 %collective-permute-done.1 = bf16[8,48,2048]{2,1,0:T(8,128)(2,1)} collective-permute-done((bf16[8,48,2048]{2,1,0:T(8,128)(2,1)}, bf16[8,48,2048]{2,1,0:T(8,128)(2,1)}, u32[]{:S(2)}, u32[]{:S(2)}) %collective-permute-start.1) | collective-permute-done | bytes 1572896 | tf_op jit(solution)/shard_map/ppermute | solution.py:10
  61.9 2.1 %broadcast_select_fusion.1 = (bf16[8,48,2048]{2,1,0:T(8,128)(2,1)S(1)}, bf16[8,48,2048]{2,1,0:T(8,128)(2,1)S(1)}) fusion(bf16[8,48,2048]{2,1,0:T(8,128)(2,1)} %all_to_all.10, bf16[8,48,2048]{2,1,0:T(8,128)(2,1)} %collective-permute-done.1, pred[]{:T(512)S(6)} %eq.55), kind=kLoop, calls=%fused_computation.24 | loop fusion | flops 1572864 | bytes 6291457 | tf_op jit(solution)/shard_map/jit(_where)/select_n | solution.py:87
  64.0 0.4 pad_maximum_fusion
  64.4 1.8 %copy-done.6 = bf16[1,2048,1024]{2,1,0:T(8,128)(2,1)S(1)} copy-done((bf16[1,2048,1024]{2,1,0:T(8,128)(2,1)S(1)}, bf16[1,2048,1024]{2,1,0:T(8,128)(2,1)}, u32[]{:S(2)}) %copy-start.6) | copy-done | bytes 4194328
  66.2 3.4 %fusion.4 = f32[768,1024]{1,0:T(8,128)S(1)} fusion(bf16[768,2048]{1,0:T(8,128)(2,1)S(1)} %bitcast.71, bf16[1,2048,1024]{2,1,0:T(8,128)(2,1)S(1)} %copy-done.6), kind=kOutput, calls=%fused_computation.4 | convolution fusion | flops 3221225472 | bytes 10485760 | tf_op jit(solution)/shard_map/dot_general | solution.py:91
  69.6 3.7 %multiply_convert_fusion = bf16[768,1024]{1,0:T(8,128)(2,1)S(1)} fusion(f32[768,1024]{1,0:T(8,128)S(1)} %fusion.4, bf16[768,2048]{1,0:T(8,128)(2,1)S(1)} %bitcast.72, bf16[1,2048,1024]{2,1,0:T(8,128)(2,1)S(1)} %copy-done.7), kind=kOutput, calls=%fused_computation.8 | convolution fusion | flops 3225944064 | bytes 12058624 | tf_op jit(solution)/shard_map/dot_general | solution.py:92
  73.4 4.8 %fusion.6 = bf16[768,2048]{1,0:T(8,128)(2,1)} fusion(bf16[768,1024]{1,0:T(8,128)(2,1)S(1)} %multiply_convert_fusion, bf16[1,1024,2048]{2,1,0:T(8,128)(2,1)S(1)} %copy-done.8), kind=kOutput, calls=%fused_computation.6 | convolution fusion | flops 3222798336 | bytes 8912896 | tf_op jit(solution)/shard_map/dot_general | solution.py:94
  78.3 1.0 copy-done.2
  79.2 0.2 copy-done.3
  79.4 0.3 multiply_convert_fusion.1
  79.7 2.2 %collective-permute-start = (bf16[30,512]{1,0:T(8,128)(2,1)S(1)}, bf16[30,512]{1,0:T(8,128)(2,1)S(1)}, u32[]{:S(2)}, u32[]{:S(2)}) collective-permute-start(bf16[30,512]{1,0:T(8,128)(2,1)S(1)} %slice.260), channel_id=1, source_target_pairs={{0,2},{2,4},{4,6},{6,8},{8,10},{10,12},{12,14},{1,3},{3,5},{5,7},{... | collective-permute-start | bytes 92168 | tf_op jit(solution)/shard_map/ppermute | solution.py:16
  82.0 0.6 collective-permute-done
  82.6 0.2 maximum_convert_fusion
  82.8 38.0 %reduce-scatter.2.cloned.1.call-done = bf16[768,1024]{1,0:T(8,128)(2,1)} async-done(((bf16[768,2048]{1,0:T(8,128)(2,1)}), bf16[768,1024]{1,0:T(8,128)(2,1)}) %reduce-scatter.2.cloned.1.call-update) | async-done | bytes 1572880 | tf_op jit(solution)/shard_map/reduce_scatter | solution.py:95
  120.8 4.7 %fusion.26 = bf16[512,512]{1,0:T(8,128)(2,1)} fusion(f32[542,512]{1,0:T(8,128)S(1)} %maximum_convert_fusion, f32[512]{0:T(512)S(1)} %bitcast.105, f32[512]{0:T(512)S(1)} %bitcast.106, f32[512]{0:T(512)S(1)} %bitcast.77, f32[512]{0:T(512)S(1)} %bitcast.78, f32[512]{0:T(512)S(1)} %bitcast.79, f32[512]{0:T(512)S(1)} %bitcast.80, f32[512]{0:T(512)S(1)} %bitcast.81, ...), kind=kLoop, calls=%fused_computation.34 | loop fusion | flops 16252928 | bytes 33093632 | tf_op jit(solution)/shard_map/convert_element_type | solution.py:51
  125.6 2.6 %add_convert_fusion = bf16[8,48,1024]{2,1,0:T(8,128)(2,1)} fusion(bf16[8,96,1024]{2,1,0:T(8,128)(2,1)} %collective-permute-done.2, s32[]{:T(128)S(6)} %select_n.31, bf16[8,96,1024]{2,1,0:T(8,128)(2,1)} %bitcast.75), kind=kLoop, calls=%fused_computation.22 | loop fusion | flops 1572864 | bytes 2359300 | tf_op jit(solution)/shard_map/convert_element_type | solution.py:101
  128.2 4.8 %all-to-all-start.1 = ((bf16[8,48,1024]{2,1,0:T(8,128)(2,1)}), bf16[8,48,1024]{2,1,0:T(8,128)(2,1)S(1)}, u32[]{:S(2)}, u32[]{:S(2)}) async-start(bf16[8,48,1024]{2,1,0:T(8,128)(2,1)} %add_convert_fusion), calls=%async_computation.2 | async-start | bytes 1572864 | tf_op jit(solution)/shard_map/all_to_all | solution.py:24
  133.0 14.0 %all-gather.2.cloned.1.call-done = bf16[512,1024]{1,0:T(8,128)(2,1)} async-done(((bf16[512,512]{1,0:T(8,128)(2,1)}), bf16[512,1024]{1,0:T(8,128)(2,1)}) %all-gather.2.cloned.1.call-update) | async-done | bytes 1048592 | tf_op jit(solution)/shard_map/all_gather | solution.py:52
  147.0 1.5 convert_reduce_fusion
  148.6 1.6 %fusion.11 = f32[512]{0:T(512)S(1)} fusion(bf16[512,1024]{1,0:T(8,128)(2,1)} %all-gather.2.cloned.1.call-done, f32[512]{0:T(512)S(1)} %broadcast_multiply_fusion), kind=kLoop, calls=%fused_computation.14 | loop fusion | flops 2096640 | bytes 1052672 | tf_op jit(solution)/shard_map/reduce_sum | solution.py:57
  150.2 2.5 %convolution_convert_fusion.1 = bf16[512,1024]{1,0:T(8,128)(2,1)} fusion(bf16[1024,1024]{1,0:T(8,128)(2,1)S(1)} %copy-done, bf16[512,1024]{1,0:T(8,128)(2,1)S(1)} %copy-done.1, f32[1024]{0:T(1024)S(1)} %copy-done.9, f32[512]{0:T(512)S(1)} %add_rsqrt_fusion, f32[512]{0:T(512)S(1)} %broadcast_multiply_fusion), kind=kOutput, calls=%fused_computation.25 | convolution fusion | flops 1078984704 | bytes 4202496 | tf_op jit(solution)/shard_map/dot_general | solution.py:61
  152.7 1.3 all-to-all-done.1
  154.0 1.3 convolution_convert_fusion.2
  (41 shorter events, 1.0 us)
Async XLA Ops:
  7.2 143.1 %copy-start = (bf16[1024,1024]{1,0:T(8,128)(2,1)S(1)}, bf16[1024,1024]{1,0:T(8,128)(2,1)}, u32[]{:S(2)}) copy-start(bf16[1024,1024]{1,0:T(8,128)(2,1)} %param.16) | copy-start | bytes 6291460
  7.2 113.6 %reduce-scatter.2.cloned.1.call-start = ((), (), s32[]{:S(2)}) async-start(), calls=%async_computation.4 | async-start | bytes 4718592 | tf_op jit(solution)/shard_map/reduce_scatter | solution.py:95
  58.1 3.8 %collective-permute-start.1 = (bf16[8,48,2048]{2,1,0:T(8,128)(2,1)}, bf16[8,48,2048]{2,1,0:T(8,128)(2,1)}, u32[]{:S(2)}, u32[]{:S(2)}) collective-permute-start(bf16[8,48,2048]{2,1,0:T(8,128)(2,1)} %all_to_all.10), channel_id=1, source_target_pairs={{0,2},{2,0},{4,6},{6,4},{8,10},{10,8},{12,14},{14,12},{1,3},{3,1},... | collective-permute-start | bytes 4718600 | tf_op jit(solution)/shard_map/ppermute | solution.py:10
  64.0 2.2 %copy-start.6 = (bf16[1,2048,1024]{2,1,0:T(8,128)(2,1)S(1)}, bf16[1,2048,1024]{2,1,0:T(8,128)(2,1)}, u32[]{:S(2)}) copy-start(bf16[1,2048,1024]{2,1,0:T(8,128)(2,1)} %param.21) | copy-start | bytes 12582916
  66.2 3.4 %copy-start.7 = (bf16[1,2048,1024]{2,1,0:T(8,128)(2,1)S(1)}, bf16[1,2048,1024]{2,1,0:T(8,128)(2,1)}, u32[]{:S(2)}) copy-start(bf16[1,2048,1024]{2,1,0:T(8,128)(2,1)} %param.22) | copy-start | bytes 12582916
  69.6 3.7 %copy-start.8 = (bf16[1,1024,2048]{2,1,0:T(8,128)(2,1)S(1)}, bf16[1,1024,2048]{2,1,0:T(8,128)(2,1)}, u32[]{:S(2)}) copy-start(bf16[1,1024,2048]{2,1,0:T(8,128)(2,1)} %param.23) | copy-start | bytes 12582916
  78.2 1.0 copy-start.2
  78.2 1.2 copy-start.3
  78.2 3.7 %copy-start.4 = (f32[31,512]{1,0:T(8,128)S(1)}, f32[31,512]{1,0:T(8,128)}, u32[]{:S(2)}) copy-start(f32[31,512]{1,0:T(8,128)} %param.14) | copy-start | bytes 190468
  78.2 68.8 %all-gather.2.cloned.1.call-start = ((), (), s32[]{:S(2)}) async-start(), calls=%async_computation.3 | async-start | bytes 1572864 | tf_op jit(solution)/shard_map/all_gather | solution.py:52
  79.7 2.9 %collective-permute-start = (bf16[30,512]{1,0:T(8,128)(2,1)S(1)}, bf16[30,512]{1,0:T(8,128)(2,1)S(1)}, u32[]{:S(2)}, u32[]{:S(2)}) collective-permute-start(bf16[30,512]{1,0:T(8,128)(2,1)S(1)} %slice.260), channel_id=1, source_target_pairs={{0,2},{2,4},{4,6},{6,8},{8,10},{10,12},{12,14},{1,3},{3,5},{5,7},{... | collective-permute-start | bytes 92168 | tf_op jit(solution)/shard_map/ppermute | solution.py:16
  120.8 4.9 %collective-permute-start.2 = (bf16[8,96,1024]{2,1,0:T(8,128)(2,1)}, bf16[8,96,1024]{2,1,0:T(8,128)(2,1)}, u32[]{:S(2)}, u32[]{:S(2)}) collective-permute-start(bf16[8,96,1024]{2,1,0:T(8,128)(2,1)} %bitcast.74), channel_id=1, source_target_pairs={{0,2},{2,0},{4,6},{6,4},{8,10},{10,8},{12,14},{14,12},{1,3},{3,1},... | collective-permute-start | bytes 4718600 | tf_op jit(solution)/shard_map/ppermute | solution.py:10
  120.8 4.7 %copy-start.5 = (f32[128,2]{0,1:T(2,128)S(1)}, f32[128,2]{0,1:T(2,128)}, u32[]{:S(2)}) copy-start(f32[128,2]{0,1:T(2,128)} %param.20) | copy-start | bytes 3076
  128.2 22.0 %copy-start.9 = (f32[1024]{0:T(1024)S(1)}, f32[1024]{0:T(1024)}, u32[]{:S(2)}) copy-start(f32[1024]{0:T(1024)} %param.15) | copy-start | bytes 12292
  128.2 25.8 %all-to-all-start.1 = ((bf16[8,48,1024]{2,1,0:T(8,128)(2,1)}), bf16[8,48,1024]{2,1,0:T(8,128)(2,1)S(1)}, u32[]{:S(2)}, u32[]{:S(2)}) async-start(bf16[8,48,1024]{2,1,0:T(8,128)(2,1)} %add_convert_fusion), calls=%async_computation.2 | async-start | bytes 1572864 | tf_op jit(solution)/shard_map/all_to_all | solution.py:24
  147.0 3.2 %copy-start.1 = (bf16[512,1024]{1,0:T(8,128)(2,1)S(1)}, bf16[512,1024]{1,0:T(8,128)(2,1)}, u32[]{:S(2)}) copy-start(bf16[512,1024]{1,0:T(8,128)(2,1)} %all-gather.2.cloned.1.call-done) | copy-start | bytes 3145732
Sparse Core Ops, SparseCore 0:
  78.3 42.3 reduce-scatter.1
  125.6 21.4 all-gather.1
where the time goes:
time: 163 us; the launch traced here: 162 us
  waiting for transfers between devices  57.6 us (35%)
  blocking collectives  44.1 us (27%)
  matrix products  17.5 us (11%)
  other arithmetic  16.9 us (10%)
  between operations  14.3 us (9%)
  starting transfers between devices  7.14 us (4%)
  local copies, waits for them, and re-layouts  4.67 us (3%)
    all_to_all x1, blocking collectives, across(): return lax.all_to_all(block, 'ep', split_axis=0, concat_axis=0, tiled=True)  44.1 us
    reduce_scatter x1, waiting for transfers between devices, on_device(): lax.psum_scatter(partial_value.astype(jnp.bfloat16), 'tp', scatter_dimens...  38 us
    all_gather x1, waiting for transfers between devices, on_device(): channels = lax.all_gather(convolved, 'tp', axis=1, tiled=True)  14 us
    all_to_all x1, starting transfers between devices, across(): return lax.all_to_all(block, 'ep', split_axis=0, concat_axis=0, tiled=True)  4.84 us
    dot_general x1, matrix products, on_device(): jnp.dot(hidden, down_w[0], preferred_element_type=jnp.float32)  4.83 us
    convert_element_type x1, other arithmetic, on_device(): convolved = total.astype(jnp.bfloat16)  4.66 us
    unnamed x21, local copies, waits for them, and re-layouts  3.85 us
    ppermute x2, waiting for transfers between devices, partner_2(): lax.ppermute(value, axis, [(i, i ^ 1 << bit) for i in range(lax.axis_size...  3.75 us
  transfers between devices with their start and end apart: 6, of which 5 were waited for; matrix products, arithmetic and copies ran while one was open for 8% of the time, Pallas kernels for 0%

commit v1 on v0

--- a/solution.py
+++ b/solution.py
@@ -1,9 +1,15 @@
+import functools
+
 import jax
 import jax.numpy as jnp
 from jax import lax
+from jax.experimental import pallas as pl
+from jax.experimental.pallas import tpu as pltpu
 from jax.sharding import PartitionSpec as P
 
 eps = 1e-06
+LANES = 128
+MESH = pl.DeviceIdType.MESH
 
 
 def partner_2(value, axis, bit):
@@ -110,7 +116,480 @@
     return (mixer_rows, routed_rows)
 
 
+def _xor(value, mask):
+    out, bit = value, 1
+    while bit <= mask:
+        if mask & bit:
+            out = out + bit - 2 * bit * lax.rem(lax.div(value, bit), 2)
+        bit *= 2
+    return out
+
+
+def _iota(shape, dim):
+    return lax.broadcasted_iota(jnp.int32, shape, dim)
+
+
+def _dot(a, b):
+    return jnp.dot(a, b, preferred_element_type=jnp.float32)
+
+
+def step_kernel(
+    chips,
+    cap,
+    pieces,
+    halo,
+    value_ref,
+    gate_ref,
+    taps_ref,
+    gain_ref,
+    wo_hbm,
+    rows_ref,
+    egain_ref,
+    routes_ref,
+    routes_t_ref,
+    rw_ref,
+    wg_hbm,
+    wu_hbm,
+    wd_hbm,
+    mixer_ref,
+    routed_ref,
+    wo,
+    wg,
+    wu,
+    wd,
+    normed,
+    picked,
+    block,
+    hid,
+    part,
+    pair_in,
+    cross_out,
+    cross_in,
+    back_out,
+    results,
+    glu,
+    halo_in,
+    conv,
+    w_sem,
+    disp_send,
+    disp_recv,
+    xf_send,
+    xf_recv,
+    cf_send,
+    cf_recv,
+    r1_send,
+    r1_recv,
+    r2_send,
+    r2_recv,
+    r3_send,
+    r3_recv,
+    ag_send,
+    ag_recv,
+    halo_send,
+    halo_recv,
+):
+    f32, bf16 = jnp.float32, jnp.bfloat16
+    ep = lax.axis_index("ep")
+    x = lax.axis_index("tp")
+    n_ep = 2 * chips
+    z, c = lax.div(ep, 2), lax.rem(ep, 2)
+    width = block.shape[-1]
+    tokens = rows_ref.shape[0]
+    length, local = value_ref.shape
+    cols = local // LANES
+    ntaps = taps_ref.shape[0]
+    split_from = max(1, chips // 2)
+    peers = [_xor(z, k) for k in range(chips)]
+
+    def dev(zd, cd, xd):
+        return {"ep": zd * 2 + cd, "tp": xd}
+
+    def remote(src, dst, send, recv, to):
+        return pltpu.make_async_remote_copy(
+            src_ref=src, dst_ref=dst, send_sem=send, recv_sem=recv, device_id=to, device_id_type=MESH
+        )
+
+    core_peer = dev(z, 1 - c, x)
+    plane_peer = dev(z, c, 1 - x)
+    after = {"ep": lax.rem(ep + 1, n_ep), "tp": x}
+    prior = {"ep": lax.rem(ep + n_ep - 1, n_ep), "tp": x}
+
+    weights = [
+        pltpu.make_async_copy(wg_hbm.at[0], wg, w_sem.at[0]),
+        pltpu.make_async_copy(wu_hbm.at[0], wu, w_sem.at[1]),
+        pltpu.make_async_copy(wd_hbm.at[0], wd, w_sem.at[2]),
+        pltpu.make_async_copy(wo_hbm, wo, w_sem.at[3]),
+    ]
+    for copy in weights:
+        copy.start()
+
+    barrier = pltpu.get_barrier_semaphore()
+    greeted = [core_peer, plane_peer, after, prior] + [dev(peers[k], c, x) for k in range(1, chips)]
+    for to in greeted:
+        pl.semaphore_signal(barrier, inc=1, device_id=to, device_id_type=MESH)
+
+    erows = -(-chips // 8) * 8
+    r0t, r1t = routes_t_ref[0:1, :], routes_t_ref[1:2, :]
+    eid = _iota((erows, tokens), 0)
+    hits_t = (r0t == eid) | (r1t == eid)
+    earlier_t = (_iota((tokens, tokens), 0) < _iota((tokens, tokens), 1)).astype(f32)
+    place_t = _dot(hits_t.astype(f32).astype(bf16), earlier_t.astype(bf16))
+    slot_t = jnp.where(hits_t, place_t, -1.0).astype(jnp.int32)
+
+    rows = rows_ref[...].astype(f32)
+    scale = lax.rsqrt(jnp.mean(rows * rows, axis=-1, keepdims=True) + eps)
+    both = (rows * scale * egain_ref[...]).astype(bf16)
+    normed[0] = both[:, :width]
+    normed[1] = both[:, width:]
+
+    sends = []
+    slots = _iota((cap, tokens), 0)
+
+    def pick(k):
+        row = jnp.sum(jnp.where(eid == peers[k], slot_t, 0), axis=0, keepdims=True)
+        return (slots == row).astype(f32).astype(bf16)
+
+    for k in range(chips - 1, 0, -1):
+        picker = pick(k)
+        if k >= split_from:
+            picked[k, 0] = _dot(picker, normed[x]).astype(bf16)
+        else:
+            for h in range(2):
+                picked[k, h] = _dot(picker, normed[h]).astype(bf16)
+    picker = pick(0)
+    for h in range(2):
+        block[z, h, c] = _dot(picker, normed[h]).astype(bf16)
+
+    pl.semaphore_wait(barrier, len(greeted))
+    for k in range(1, chips):
+        to = dev(peers[k], c, x)
+        if k >= split_from:
+            copies = [
+                remote(picked.at[k, 0], block.at[z, x, c], disp_send.at[k, 0], disp_recv.at[z, 0], to)
+            ]
+        else:
+            copies = [
+                remote(
+                    picked.at[k, h], block.at[z, h, c], disp_send.at[k, h], disp_recv.at[z, h], to
+                )
+                for h in range(2)
+            ]
+        for copy in copies:
+            copy.start()
+        sends.extend(copies)
+
+    def start(copy):
+        copy.start()
+        sends.append(copy)
+
+    def to_core(k, h, sem):
+        zs = peers[k]
+        start(
+            remote(
+                block.at[zs, h, c],
+                block.at[zs, h, c],
+                cf_send.at[k, sem],
+                cf_recv.at[k, sem],
+                core_peer,
+            )
+        )
+
+    def from_core(k, h, sem):
+        zs = peers[k]
+        remote(
+            block.at[zs, h, 1 - c],
+            block.at[zs, h, 1 - c],
+            cf_send.at[k, sem],
+            cf_recv.at[k, sem],
+            core_peer,
+        ).wait_recv()
+
+    def arrived(k, h, sem):
+        zs = peers[k]
+        remote(
+            block.at[zs, h, c],
+            block.at[zs, h, c],
+            disp_send.at[k, sem],
+            disp_recv.at[zs, sem],
+            dev(zs, c, x),
+        ).wait_recv()
+
+    def experts(k):
+        zs = peers[k]
+        a0 = block[zs, 0].reshape(2 * cap, width)
+        a1 = block[zs, 1].reshape(2 * cap, width)
+        units = hid.shape[1]
+        step = min(units, 256)
+        for j in range(0, units, step):
+            gate = _dot(a0, wg[:width, j : j + step]) + _dot(a1, wg[width:, j : j + step])
+            up = _dot(a0, wu[:width, j : j + step]) + _dot(a1, wu[width:, j : j + step])
+            hid[:, j : j + step] = (gate * jax.nn.sigmoid(gate) * up).astype(bf16)
+        h_all = hid[...]
+        for h in range(2):
+            for j in range(0, width, step):
+                out = _dot(h_all, wd[:, h * width + j : h * width + j + step]).astype(bf16)
+                part[k, 0, h, :, j : j + step] = out[:cap]
+                part[k, 1, h, :, j : j + step] = out[cap:]
+        start(remote(part.at[k, 1 - c], pair_in.at[k], r1_send.at[k], r1_recv.at[k], core_peer))
+
+    def pair_sum(k):
+        remote(
+            part.at[k, 1 - c], pair_in.at[k], r1_send.at[k], r1_recv.at[k], core_peer
+        ).wait_recv()
+        total = part[k, c, 1 - x].astype(f32) + pair_in[k, 1 - x].astype(f32)
+        cross_out[k] = total.astype(bf16)
+        start(remote(cross_out.at[k], cross_in.at[k], r2_send.at[k], r2_recv.at[k], plane_peer))
+
+    def plane_sum(k):
+        remote(
+            cross_out.at[k], cross_in.at[k], r2_send.at[k], r2_recv.at[k], plane_peer
+        ).wait_recv()
+        total = part[k, c, x].astype(f32) + pair_in[k, x].astype(f32) + cross_in[k].astype(f32)
+        if k == 0:
+            results[z] = total.astype(bf16)
+        else:
+            back_out[k] = total.astype(bf16)
+            start(
+                remote(
+                    back_out.at[k],
+                    results.at[z],
+                    r3_send.at[k],
+                    r3_recv.at[z],
+                    dev(peers[k], c, x),
+                )
+            )
+
+    for h in range(2):
+        to_core(0, h, h)
+
+    for i in range(cols):
+        part_cols = slice(i * LANES, (i + 1) * LANES)
+        gated = value_ref[:, part_cols].astype(f32) * jax.nn.sigmoid(
+            gate_ref[:, part_cols].astype(f32)
+        )
+        glu[i, halo:, :] = gated.astype(bf16).astype(f32)
+    start(
+        remote(
+            glu.at[:, pl.ds(length, halo)], halo_in, halo_send.at[0], halo_recv.at[0], after
+        )
+    )
+
+    for h in range(2):
+        from_core(0, h, h)
+    for copy in weights[:3]:
+        copy.wait()
+    experts(0)
+
+    remote(
+        glu.at[:, pl.ds(length, halo)], halo_in, halo_send.at[0], halo_recv.at[0], after
+    ).wait_recv()
+    glu[:, :halo, :] = jnp.where(ep > 0, halo_in[...], 0.0)
+    tile = 64 if length % 64 == 0 else length
+    for i in range(cols):
+
+        def conv_tile(r, carry):
+            r0 = pl.multiple_of(r * tile, tile)
+            total = jnp.zeros((tile, LANES), f32)
+            for k in range(ntaps):
+                total = (
+                    total
+                    + taps_ref[k : k + 1, i * LANES : (i + 1) * LANES]
+                    * glu[i, pl.ds(r0 + (k + halo - ntaps + 1), tile), :]
+                )
+            conv[x, pl.ds(r0, tile), i * LANES : (i + 1) * LANES] = total.astype(bf16)
+            return carry
+
+        lax.fori_loop(0, length // tile, conv_tile, 0)
+
+    rows_per = length // pieces
+
+    def gather_copy(p):
+        own = conv.at[x, pl.ds(p * rows_per, rows_per)]
+        return remote(own, own, ag_send.at[p], ag_recv.at[p], plane_peer)
+
+    def gather_some(lo, hi):
+        for p in range(lo, hi):
+            start(gather_copy(p))
+
+    gather_some(0, pieces // 2)
+    for k in range(1, split_from):
+        for h in range(2):
+            arrived(k, h, h)
+            to_core(k, h, h)
+    pair_sum(0)
+    done = 1
+    for k in range(1, split_from):
+        for h in range(2):
+            from_core(k, h, h)
+        experts(k)
+    for k in range(split_from, chips):
+        arrived(k, x, 0)
+        zs = peers[k]
+        start(
+            remote(block.at[zs, x, c], block.at[zs, x, c], xf_send.at[k], xf_recv.at[k], plane_peer)
+        )
+        to_core(k, x, 0)
+    gather_some(pieces // 2, pieces)
+    plane_sum(0)
+    for k in range(1, split_from):
+        pair_sum(k)
+    for k in range(split_from, chips):
+        zs = peers[k]
+        remote(
+            block.at[zs, 1 - x, c], block.at[zs, 1 - x, c], xf_send.at[k], xf_recv.at[k], plane_peer
+        ).wait_recv()
+        to_core(k, 1 - x, 1)
+        from_core(k, x, 0)
+        from_core(k, 1 - x, 1)
+        experts(k)
+        if k > split_from:
+            pair_sum(k - 1)
+    for k in range(1, split_from):
+        plane_sum(k)
+    pair_sum(chips - 1)
+
+    weights[3].wait()
+    for p in range(pieces):
+        other = conv.at[1 - x, pl.ds(p * rows_per, rows_per)]
+        remote(other, other, ag_send.at[p], ag_recv.at[p], plane_peer).wait_recv()
+        here = slice(p * rows_per, (p + 1) * rows_per)
+        lo, hi = conv[0, here, :].astype(f32), conv[1, here, :].astype(f32)
+        count = 2 * local
+        mean = (
+            jnp.sum(lo, axis=-1, keepdims=True) + jnp.sum(hi, axis=-1, keepdims=True)
+        ) / count
+        lo, hi = lo - mean, hi - mean
+        var = (
+            jnp.sum(lo * lo, axis=-1, keepdims=True) + jnp.sum(hi * hi, axis=-1, keepdims=True)
+        ) / count
+        scale = lax.rsqrt(var + eps)
+        lo = lo * scale * gain_ref[:, :local]
+        hi = hi * scale * gain_ref[:, local:]
+        lo = (lo * jax.nn.sigmoid(lo)).astype(bf16)
+        hi = (hi * jax.nn.sigmoid(hi)).astype(bf16)
+        mixer_ref[here, :] = (_dot(lo, wo[:local, :]) + _dot(hi, wo[local:, :])).astype(bf16)
+
+    for k in range(split_from, chips):
+        plane_sum(k)
+
+    lane = _iota((tokens, LANES), 1)
+    r0, r1 = routes_ref[:, 0:1], routes_ref[:, 1:2]
+    hits = ((r0 == lane) | (r1 == lane)).astype(f32).astype(bf16)
+    earlier = (_iota((tokens, tokens), 1) < _iota((tokens, tokens), 0)).astype(f32).astype(bf16)
+    place = _dot(earlier, hits)
+    all_slots = _iota((tokens, chips * cap), 1)
+    comb = jnp.zeros((tokens, chips * cap), f32)
+    for j, r in enumerate((r0, r1)):
+        at = jnp.sum(jnp.where(lane == r, place, 0.0), axis=1, keepdims=True).astype(jnp.int32)
+        comb = comb + jnp.where(all_slots == r * cap + at, rw_ref[:, j : j + 1], 0.0)
+    head = comb.astype(bf16)
+    tail = (comb - head.astype(f32)).astype(bf16)
+    for k in range(1, chips):
+        zs = peers[k]
+        remote(
+            back_out.at[k], results.at[zs], r3_send.at[k], r3_recv.at[zs], dev(zs, c, x)
+        ).wait_recv()
+    found = results[...].reshape(chips * cap, width)
+    routed_ref[...] = (_dot(head, found) + _dot(tail, found)).astype(bf16)
+    for copy in sends:
+        copy.wait_send()
+
+
+def one_kernel(
+    value_in,
+    gate_in,
+    conv_taps,
+    chan_gain,
+    out_weight,
+    second_rows,
+    expert_gain,
+    routes,
+    route_weights,
+    gate_w,
+    up_w,
+    down_w,
+):
+    chips = lax.axis_size("ep") // 2
+    tokens, model = second_rows.shape
+    top = routes.shape[1]
+    width = model // 2
+    cap = 2 * max(1, min(tokens // 2, 3 * tokens * top // (4 * chips)))
+    length, local = value_in.shape
+    units = gate_w.shape[2]
+    halo = -(-(conv_taps.shape[0] - 1) // 8) * 8
+    pieces = 4
+    bf16, f32 = jnp.bfloat16, jnp.float32
+    vmem = pl.BlockSpec(memory_space=pltpu.VMEM)
+    hbm = pl.BlockSpec(memory_space=pl.ANY)
+    dma = pltpu.SemaphoreType.DMA
+    scratch = [
+        pltpu.VMEM(out_weight.shape, bf16),
+        pltpu.VMEM(gate_w.shape[1:], bf16),
+        pltpu.VMEM(up_w.shape[1:], bf16),
+        pltpu.VMEM(down_w.shape[1:], bf16),
+        pltpu.VMEM((2, tokens, width), bf16),
+        pltpu.VMEM((chips, 2, cap, width), bf16),
+        pltpu.VMEM((chips, 2, 2, cap, width), bf16),
+        pltpu.VMEM((2 * cap, units), bf16),
+        pltpu.VMEM((chips, 2, 2, cap, width), bf16),
+        pltpu.VMEM((chips, 2, cap, width), bf16),
+        pltpu.VMEM((chips, cap, width), bf16),
+        pltpu.VMEM((chips, cap, width), bf16),
+        pltpu.VMEM((chips, cap, width), bf16),
+        pltpu.VMEM((chips, cap, width), bf16),
+        pltpu.VMEM((local // LANES, halo + length, LANES), f32),
+        pltpu.VMEM((local // LANES, halo, LANES), f32),
+        pltpu.VMEM((2, length, local), bf16),
+        dma((4,)),
+        dma((chips, 2)),
+        dma((chips, 2)),
+        dma((chips,)),
+        dma((chips,)),
+        dma((chips, 2)),
+        dma((chips, 2)),
+        dma((chips,)),
+        dma((chips,)),
+        dma((chips,)),
+        dma((chips,)),
+        dma((chips,)),
+        dma((chips,)),
+        dma((pieces,)),
+        dma((pieces,)),
+        dma((1,)),
+        dma((1,)),
+    ]
+    return pl.pallas_call(
+        functools.partial(step_kernel, chips, cap, pieces, halo),
+        out_shape=(
+            jax.ShapeDtypeStruct((length, out_weight.shape[1]), bf16),
+            jax.ShapeDtypeStruct((tokens, width), bf16),
+        ),
+        in_specs=[vmem] * 4 + [hbm] + [vmem] * 5 + [hbm] * 3,
+        out_specs=(vmem, vmem),
+        scratch_shapes=scratch,
+        compiler_params=pltpu.CompilerParams(
+            collective_id=0, has_side_effects=True, vmem_limit_bytes=60 * 1024 * 1024
+        ),
+    )(
+        value_in,
+        gate_in,
+        conv_taps,
+        chan_gain.reshape(1, -1),
+        out_weight,
+        second_rows,
+        expert_gain.reshape(1, -1),
+        routes,
+        routes.T,
+        route_weights,
+        gate_w,
+        up_w,
+        down_w,
+    )
+
+
 def solution(mesh):
+    chips = mesh.shape["ep"] // 2
+    paired = mesh.shape["tp"] == 2 and chips > 1 and chips & (chips - 1) == 0
     placed = (
         P(("grp", "ep"), "tp"),
         P(("grp", "ep"), "tp"),
@@ -126,7 +605,7 @@
         P("ep", "tp", None),
     )
     return jax.shard_map(
-        on_device,
+        one_kernel if paired else on_device,
         mesh=mesh,
         in_specs=placed,
         out_specs=(P(("grp", "ep"), "tp"), P(("grp", "ep"), "tp")),

time: 163 us -> 83.2 us (0.51)
  the two profiles are of different devices: /device:TPU:0 before, /device:TPU:20 now
where the time goes in v1:
time: 83.2 us; the launch traced here: 83 us
  Pallas kernels  75.6 us (91%)
  local copies, waits for them, and re-layouts  6.76 us (8%)
    pallas_call x1, Pallas kernels, one_kernel(): pl.pallas_call(functools.partial(step_kernel, chips, cap, pieces, halo),...  75.6 us
    unnamed x4, local copies, waits for them, and re-layouts  6.76 us

profile of v1, /device:TPU:20, one launch (start us, length us, event | category | flops | bytes accessed | tf_op | source)
XLA Modules:
  0.0 83.0 jit_solution(1788874009362563026)
XLA Ops:
  0.6 1.4 %copy.15.rw_ref = f32[128,2]{1,0:T(8,128)} copy(f32[128,2]{0,1:T(2,128)} %param.20) | data formatting | bytes 2048 | tf_op args[8]
  2.0 1.4 %copy.14.routes_ref = s32[128,2]{1,0:T(8,128)} copy(s32[128,2]{0,1:T(2,128)} %param.19) | data formatting | bytes 2048 | tf_op args[7]
  3.5 75.6 %shard_map.131 = (bf16[512,1024]{1,0:T(8,128)(2,1)}, bf16[128,1024]{1,0:T(8,128)(2,1)}) custom-call(bf16[512,512]{1,0:T(8,128)(2,1)} %value_ref.1, bf16[512,512]{1,0:T(8,128)(2,1)} %gate_ref.1, f32[31,512]{1,0:T(8,128)} %taps_ref.1, f32[1,1024]{1,0:T(1,128)} %bitcast.4, bf16[1024,1024]{1,0:T(8,128)(2,1)} %wo_hbm.1, bf16[128,2048]{1,0:T(8,128)(2,1)} %rows_ref.1, ...), custom_call_target="tpu_custom_call" | custom-call | tf_op jit(solution)/shard_map/pallas_call | solution.py:561
  79.0 2.3 %copy.18 = bf16[512,1024]{1,0:T(8,128)(2,1)} copy(bf16[512,1024]{1,0:T(8,128)(2,1)} %get-tuple-element.4) | data formatting | bytes 2097152
  81.3 1.7 %copy.19 = bf16[128,1024]{1,0:T(8,128)(2,1)} copy(bf16[128,1024]{1,0:T(8,128)(2,1)} %get-tuple-element.5) | data formatting | bytes 524288

commit v2 on v1

--- a/solution.py
+++ b/solution.py
@@ -145,9 +145,8 @@
     wo_hbm,
     rows_ref,
     egain_ref,
-    routes_ref,
     routes_t_ref,
-    rw_ref,
+    rw_t_ref,
     wg_hbm,
     wu_hbm,
     wd_hbm,
@@ -261,11 +260,25 @@
         block[z, h, c] = _dot(picker, normed[h]).astype(bf16)
 
     pl.semaphore_wait(barrier, len(greeted))
-    for k in range(1, chips):
+    subs = 2 if cap % 32 == 0 else 1
+    far = list(range(split_from, chips))
+    near = list(range(1, split_from))
+
+    def sub(s):
+        return pl.ds(s * (cap // subs), cap // subs)
+
+    for k in far + near:
         to = dev(peers[k], c, x)
         if k >= split_from:
             copies = [
-                remote(picked.at[k, 0], block.at[z, x, c], disp_send.at[k, 0], disp_recv.at[z, 0], to)
+                remote(
+                    picked.at[k, 0, sub(s)],
+                    block.at[z, x, c, sub(s)],
+                    disp_send.at[k, s],
+                    disp_recv.at[z, s],
+                    to,
+                )
+                for s in range(subs)
             ]
         else:
             copies = [
@@ -282,36 +295,20 @@
         copy.start()
         sends.append(copy)
 
-    def to_core(k, h, sem):
-        zs = peers[k]
-        start(
-            remote(
-                block.at[zs, h, c],
-                block.at[zs, h, c],
-                cf_send.at[k, sem],
-                cf_recv.at[k, sem],
-                core_peer,
-            )
-        )
-
-    def from_core(k, h, sem):
-        zs = peers[k]
+    whole = pl.ds(0, cap)
+
+    def to_core(k, h, sem, rows_of=whole):
+        here = block.at[peers[k], h, c, rows_of]
+        start(remote(here, here, cf_send.at[k, sem], cf_recv.at[k, sem], core_peer))
+
+    def from_core(k, h, sem, rows_of=whole):
+        here = block.at[peers[k], h, 1 - c, rows_of]
+        remote(here, here, cf_send.at[k, sem], cf_recv.at[k, sem], core_peer).wait_recv()
+
+    def arrived(k, h, sem, rows_of=whole):
+        here = block.at[peers[k], h, c, rows_of]
         remote(
-            block.at[zs, h, 1 - c],
-            block.at[zs, h, 1 - c],
-            cf_send.at[k, sem],
-            cf_recv.at[k, sem],
-            core_peer,
-        ).wait_recv()
-
-    def arrived(k, h, sem):
-        zs = peers[k]
-        remote(
-            block.at[zs, h, c],
-            block.at[zs, h, c],
-            disp_send.at[k, sem],
-            disp_recv.at[zs, sem],
-            dev(zs, c, x),
+            here, here, disp_send.at[k, sem], disp_recv.at[peers[k], sem], dev(peers[k], c, x)
         ).wait_recv()
 
     def experts(k):
@@ -411,42 +408,42 @@
         for p in range(lo, hi):
             start(gather_copy(p))
 
-    gather_some(0, pieces // 2)
-    for k in range(1, split_from):
+    gather_some(0, 1)
+    for k in far:
+        for s in range(subs):
+            arrived(k, x, s, sub(s))
+            here = block.at[peers[k], x, c, sub(s)]
+            start(remote(here, here, xf_send.at[k, s], xf_recv.at[k, s], plane_peer))
+            to_core(k, x, s, sub(s))
+    pair_sum(0)
+    for k in near:
         for h in range(2):
             arrived(k, h, h)
             to_core(k, h, h)
-    pair_sum(0)
-    done = 1
-    for k in range(1, split_from):
+    for k in near:
         for h in range(2):
             from_core(k, h, h)
         experts(k)
-    for k in range(split_from, chips):
-        arrived(k, x, 0)
-        zs = peers[k]
-        start(
-            remote(block.at[zs, x, c], block.at[zs, x, c], xf_send.at[k], xf_recv.at[k], plane_peer)
-        )
-        to_core(k, x, 0)
-    gather_some(pieces // 2, pieces)
+    for k in far:
+        for s in range(subs):
+            here = block.at[peers[k], 1 - x, c, sub(s)]
+            remote(here, here, xf_send.at[k, s], xf_recv.at[k, s], plane_peer).wait_recv()
+            to_core(k, 1 - x, subs + s, sub(s))
+        if k == far[0]:
+            for q in near:
+                pair_sum(q)
+        for s in range(subs):
+            from_core(k, x, s, sub(s))
+            from_core(k, 1 - x, subs + s, sub(s))
+        experts(k)
+        if k > far[0]:
+            plane_sum(k - 1)
+        pair_sum(k)
+    gather_some(1, pieces)
+    for k in near:
+        plane_sum(k)
+    plane_sum(chips - 1)
     plane_sum(0)
-    for k in range(1, split_from):
-        pair_sum(k)
-    for k in range(split_from, chips):
-        zs = peers[k]
-        remote(
-            block.at[zs, 1 - x, c], block.at[zs, 1 - x, c], xf_send.at[k], xf_recv.at[k], plane_peer
-        ).wait_recv()
-        to_core(k, 1 - x, 1)
-        from_core(k, x, 0)
-        from_core(k, 1 - x, 1)
-        experts(k)
-        if k > split_from:
-            pair_sum(k - 1)
-    for k in range(1, split_from):
-        plane_sum(k)
-    pair_sum(chips - 1)
 
     weights[3].wait()
     for p in range(pieces):
@@ -469,11 +466,13 @@
         hi = (hi * jax.nn.sigmoid(hi)).astype(bf16)
         mixer_ref[here, :] = (_dot(lo, wo[:local, :]) + _dot(hi, wo[local:, :])).astype(bf16)
 
-    for k in range(split_from, chips):
-        plane_sum(k)
-
     lane = _iota((tokens, LANES), 1)
-    r0, r1 = routes_ref[:, 0:1], routes_ref[:, 1:2]
+    index = _iota((8, tokens), 0)
+    rows_named = jnp.where(index == 0, r0t, 0).astype(f32) + jnp.where(index == 1, r1t, 0).astype(f32)
+    for j in range(2):
+        rows_named = rows_named + jnp.where(index == 2 + j, rw_t_ref[j : j + 1, :], 0.0)
+    named = jnp.transpose(rows_named)
+    r0, r1 = (named[:, j : j + 1].astype(jnp.int32) for j in range(2))
     hits = ((r0 == lane) | (r1 == lane)).astype(f32).astype(bf16)
     earlier = (_iota((tokens, tokens), 1) < _iota((tokens, tokens), 0)).astype(f32).astype(bf16)
     place = _dot(earlier, hits)
@@ -481,7 +480,7 @@
     comb = jnp.zeros((tokens, chips * cap), f32)
     for j, r in enumerate((r0, r1)):
         at = jnp.sum(jnp.where(lane == r, place, 0.0), axis=1, keepdims=True).astype(jnp.int32)
-        comb = comb + jnp.where(all_slots == r * cap + at, rw_ref[:, j : j + 1], 0.0)
+        comb = comb + jnp.where(all_slots == r * cap + at, named[:, 2 + j : 3 + j], 0.0)
     head = comb.astype(bf16)
     tail = (comb - head.astype(f32)).astype(bf16)
     for k in range(1, chips):
@@ -543,10 +542,10 @@
         dma((4,)),
         dma((chips, 2)),
         dma((chips, 2)),
-        dma((chips,)),
-        dma((chips,)),
         dma((chips, 2)),
         dma((chips, 2)),
+        dma((chips, 4)),
+        dma((chips, 4)),
         dma((chips,)),
         dma((chips,)),
         dma((chips,)),
@@ -564,7 +563,7 @@
             jax.ShapeDtypeStruct((length, out_weight.shape[1]), bf16),
             jax.ShapeDtypeStruct((tokens, width), bf16),
         ),
-        in_specs=[vmem] * 4 + [hbm] + [vmem] * 5 + [hbm] * 3,
+        in_specs=[vmem] * 4 + [hbm] + [vmem] * 4 + [hbm] * 3,
         out_specs=(vmem, vmem),
         scratch_shapes=scratch,
         compiler_params=pltpu.CompilerParams(
@@ -578,9 +577,8 @@
         out_weight,
         second_rows,
         expert_gain.reshape(1, -1),
-        routes,
         routes.T,
-        route_weights,
+        route_weights.T,
         gate_w,
         up_w,
         down_w,

time: 83.2 us -> 69.1 us (0.83)
  the two profiles are of different devices: /device:TPU:20 before, /device:TPU:0 now
where the time goes in v2:
time: 69.1 us; the launch traced here: 68.1 us
  Pallas kernels  63.5 us (92%)
  local copies, waits for them, and re-layouts  3.93 us (6%)
    pallas_call x1, Pallas kernels, one_kernel(): pl.pallas_call(functools.partial(step_kernel, chips, cap, pieces, halo),...  63.5 us
    unnamed x2, local copies, waits for them, and re-layouts  3.93 us

profile of v2, /device:TPU:0, one launch (start us, length us, event | category | flops | bytes accessed | tf_op | source)
XLA Modules:
  0.0 68.1 jit_solution(18412623000148464109)
XLA Ops:
  0.6 63.5 %shard_map.131 = (bf16[512,1024]{1,0:T(8,128)(2,1)}, bf16[128,1024]{1,0:T(8,128)(2,1)}) custom-call(bf16[512,512]{1,0:T(8,128)(2,1)} %value_ref.1, bf16[512,512]{1,0:T(8,128)(2,1)} %gate_ref.1, f32[31,512]{1,0:T(8,128)} %taps_ref.1, f32[1,1024]{1,0:T(1,128)} %bitcast.5, bf16[1024,1024]{1,0:T(8,128)(2,1)} %wo_hbm.1, bf16[128,2048]{1,0:T(8,128)(2,1)} %rows_ref.1, ...), custom_call_target="tpu_custom_call" | custom-call | tf_op jit(solution)/shard_map/pallas_call | solution.py:560
  64.1 2.3 %copy.16 = bf16[512,1024]{1,0:T(8,128)(2,1)} copy(bf16[512,1024]{1,0:T(8,128)(2,1)} %get-tuple-element.4) | data formatting | bytes 2097152
  66.4 1.7 %copy.17 = bf16[128,1024]{1,0:T(8,128)(2,1)} copy(bf16[128,1024]{1,0:T(8,128)(2,1)} %get-tuple-element.5) | data formatting | bytes 524288
